TPU v7x, 32 devices: a whole 2x2x4 slice. The times are simulated.
32 devices in a mesh: ep: 8 (over z, x), tp: 4 (over y, core).
Axes of the slice: x: 2, y: 2, z: 4, core: 2. Of those that a mesh axis runs over, the one named last changes fastest.
Arguments:
- tokens: bfloat16 [2048, 2048], P('ep', 'tp'), may hold values from -6 to 6
- row_ids: int32 [2048, 16], P('ep'), may hold values from 0 to 32767, as said below
- row_gates: float32 [2048, 16], P('ep'), may hold values from 0.02 to 0.5
- key_table: bfloat16 [32768, 2048], P('ep', 'tp'), may hold values from -0.125 to 0.125
- value_table: bfloat16 [32768, 2048], P('ep', 'tp'), may hold values from -14 to 14
- norm_gain: float32 [2048], P('tp'), may hold values from 0.1 to 1.9
Outputs:
- output: bfloat16 [2048, 2048], P('ep', 'tp')
Inputs may be any that keep to these rules, and one draw needn't show every extreme that they name: `row_ids`: table row r belongs to index r // 4096 of ep. The 256 tokens of one index of ep choose at most 1536 rows belonging to any one index, exactly 1536 from some index, and at least one from every index.
All inputs are finite; a program needn't handle non-finite values.
Results may differ from a plain program's by a relative error of at most 0.0065.
Values may be sent and summed in bfloat16 or wider, within the bound.
A program may use at most 64 MiB of HBM per device.

v0:
```python
import functools

import jax
import jax.numpy as jnp
from jax import lax
from jax.experimental import pallas as pl
from jax.experimental.pallas import tpu as pltpu
from jax.sharding import PartitionSpec as P

ROW = 256
LANES = 128
MESH = pl.DeviceIdType.MESH


def cycle_of(n):
    x = 1
    while 4 * x * x <= n:
        x *= 2
    z = n // x
    if x == 1 or z % 2:
        return list(range(n))
    out = []
    for row in range(z):
        cols = range(1, x) if row % 2 == 0 else range(x - 1, 0, -1)
        out += [row * x + col for col in cols]
    return out + [row * x for row in range(z - 1, -1, -1)]


def look(table, i):
    n = len(table)
    total = 0
    for k, v in enumerate(table):
        total = total + v * ((n * n - (i - k) * (i - k)) // (n * n))
    return total


def greet(n, tps, me, order):
    pos = look([order.index(i) for i in range(n)], me)
    right = look(order, lax.rem(pos + 1, n))
    left = look(order, lax.rem(pos + n - 1, n))
    mine = lax.axis_index("tp")
    barrier = pltpu.get_barrier_semaphore()
    for peer in (left, right):
        pl.semaphore_signal(barrier, inc=1, device_id=(peer, mine), device_id_type=MESH)
    for k in range(1, tps):
        pl.semaphore_signal(
            barrier, inc=1, device_id=(me, lax.rem(mine + k, tps)), device_id_type=MESH
        )
    pl.semaphore_wait(barrier, 2 + tps - 1)
    return pos, right, left, mine


def remote(src, dst, send, recv, device):
    return pltpu.make_async_remote_copy(
        src_ref=src, dst_ref=dst, send_sem=send, recv_sem=recv, device_id=device, device_id_type=MESH
    )


def kernel(n, tps, picks, order, *refs):
    x_ref, meta_ref, key_hbm, value_hbm, gain_ref, out_ref = refs[:6]
    key_ref, value_ref, xall, metas, s_ref, part, got_ref, hid_ref, w_ref = refs[6:15]
    out_total, sent, came, sq_ref, sq_got = refs[15:20]
    xs, xr, ms, mr, ps, pr, ss, sr, qs, qr, kv = refs[20:]
    block, width = x_ref.shape
    half = block // 2
    experts = key_ref.shape[0]
    lines = meta_ref.shape[1] // 2
    rows = half // 2
    cuts = ss.shape[2]
    wide_out = width // cuts
    key_copy = pltpu.make_async_copy(key_hbm, key_ref, kv.at[0])
    value_copy = pltpu.make_async_copy(value_hbm, value_ref, kv.at[1])
    key_copy.start()
    me = lax.axis_index("ep")
    pos, right, left, mine = greet(n, tps, me, order)
    base = me * experts
    peers = (right, left)

    def x_copy(d, step, c, first=False):
        at = pl.ds(d * half + c * rows, rows)
        src = x_ref.at[at] if first else xall.at[step, at]
        return remote(
            src, xall.at[step + 1, at], xs.at[d, step, c], xr.at[d, step, c], (peers[d], mine)
        )

    def m_copy(d, step, first=False):
        src = meta_ref.at[d] if first else metas.at[step, d]
        return remote(src, metas.at[step + 1, d], ms.at[d, step], mr.at[d, step], (peers[d], mine))

    def p_copy(s, k):
        return remote(
            part.at[s],
            got_ref.at[s, k - 1],
            ps.at[s, k - 1],
            pr.at[s, k - 1],
            (me, lax.rem(mine + k, tps)),
        )

    for c in range(2):
        for d in (0, 1):
            x_copy(d, 0, c, True).start()
            if c == 0:
                m_copy(d, 0, True).start()
    xall[0] = x_ref[...]
    metas[0] = meta_ref[...]
    value_copy.start()
    key_copy.wait()

    per_half = LANES // picks
    sub = lax.broadcasted_iota(jnp.int32, (per_half, LANES), 0)
    lane = lax.broadcasted_iota(jnp.int32, (per_half, LANES), 1)
    own_lane = sub == lane // picks
    wide = min(512, experts)

    def pass_on(s, c):
        for d in (0, 1):
            x_copy(d, s - 1, c).wait_recv()

            @pl.when(s < n - 1)
            def _():
                x_copy(d, s, c).start()

            if c == 0:
                m_copy(d, s - 1).wait_recv()

                @pl.when(s < n - 1)
                def _():
                    m_copy(d, s).start()

    def choose(s):
        for d in (0, 1):
            all_ids = metas[s, d, :lines, :].astype(jnp.int32) - base
            for h2 in range(ROW // LANES):
                out = []
                for r in range(lines):
                    ids = all_ids[r : r + 1, h2 * LANES : (h2 + 1) * LANES]
                    ids = jnp.broadcast_to(ids, (per_half, LANES))
                    owned = (ids >= 0) & (ids < experts)
                    hi = jnp.where(owned, ids >> 7, -1)
                    lo = jnp.where(owned, ids & (LANES - 1), 0)
                    row = d * half + r * (ROW // picks) + h2 * per_half
                    acc = jnp.zeros((per_half, LANES), jnp.float32)
                    for h in range(experts // LANES):
                        tile = s_ref[row : row + per_half, h * LANES : (h + 1) * LANES]
                        acc = jnp.where(hi == h, jnp.take_along_axis(tile, lo, axis=1), acc)
                    out.append(jnp.sum(jnp.where(own_lane, acc, 0.0), axis=0, keepdims=True))
                part[s, d * lines : (d + 1) * lines, h2 * LANES : (h2 + 1) * LANES] = (
                    jnp.concatenate(out, axis=0)
                )
        for k in range(1, tps):
            p_copy(s, k).start()

    def score_step(s, carry):
        @pl.when((s >= 1) & (s < n))
        def _():
            pass_on(s, 0)

        @pl.when(s >= 1)
        def _():
            choose(s - 1)

        @pl.when((s >= 1) & (s < n))
        def _():
            pass_on(s, 1)

        @pl.when(s < n)
        def _():
            for c in range(experts // wide):
                s_ref[:, c * wide : (c + 1) * wide] = lax.dot_general(
                    xall[s],
                    key_ref[c * wide : (c + 1) * wide, :],
                    (((1,), (1,)), ((), ())),
                    preferred_element_type=jnp.float32,
                )

        return carry

    lax.fori_loop(0, n + 1, score_step, 0)
    value_copy.wait()

    per = ROW // picks
    tall = experts // ROW * per
    lane_token = lax.broadcasted_iota(jnp.int32, (lines, ROW), 1) // picks
    tall_iota = lax.broadcasted_iota(jnp.int32, (tall, ROW), 0)
    lo_iota = lax.broadcasted_iota(jnp.int32, (ROW, ROW), 0)

    def copy(d, s, c):
        return remote(
            sent.at[s, d, c], came.at[s, d, c], ss.at[d, s, c], sr.at[d, s, c], (peers[d], mine)
        )

    def mix_step(s, carry):
        slot = lax.rem(s + 1, n)
        total = part[slot]
        for k in range(1, tps):
            p_copy(slot, k).wait()
            total = total + got_ref[slot, k - 1]
        hid_ref[...] = 0.5 * total * (1.0 + lax.erf(total * (0.5**0.5)))
        for d in (0, 1):
            ids = metas[slot, d, :lines, :].astype(jnp.int32) - base
            owned = (ids >= 0) & (ids < experts)
            codes = jnp.where(owned, (ids >> 8) * per + lane_token, -1)
            los = ids & (ROW - 1)
            hs = hid_ref[d * lines : (d + 1) * lines, :] * metas[slot, d, lines:, :]
            for r in range(lines):
                code, lo, h = codes[r : r + 1, :], los[r : r + 1, :], hs[r : r + 1, :]
                a = jnp.where(tall_iota == code, h, 0.0).astype(jnp.bfloat16)
                b = jnp.where(lo_iota == lo, 1.0, 0.0).astype(jnp.bfloat16)
                w = lax.dot_general(
                    a, b, (((1,), (1,)), ((), ())), preferred_element_type=jnp.float32
                ).astype(jnp.bfloat16)
                row = d * half + r * per
                for c in range(experts // ROW):
                    w_ref[row : row + per, c * ROW : (c + 1) * ROW] = w[c * per : (c + 1) * per, :]
        for c in range(cuts):
            cols = slice(c * wide_out, (c + 1) * wide_out)
            out_total[:, cols] = jnp.dot(
                w_ref[...], value_ref[:, cols], preferred_element_type=jnp.float32
            )
            for d in (0, 1):
                at = slice(d * half, (d + 1) * half)

                @pl.when(s >= 1)
                def _():
                    copy(d, s - 1, c).wait_recv()
                    out_total[at, cols] = out_total[at, cols] + came[s - 1, d, c].astype(
                        jnp.float32
                    )

                @pl.when(s < n - 1)
                def _():
                    sent[s, d, c] = out_total[at, cols].astype(jnp.bfloat16)
                    copy(d, s, c).start()

        return carry

    lax.fori_loop(0, n, mix_step, 0)
    mixed = out_total[...]
    ones = jnp.ones((8, width), jnp.float32)
    square = lax.dot_general(
        ones,
        mixed * mixed,
        (((1,), (1,)), ((), ())),
        precision=lax.Precision.HIGHEST,
        preferred_element_type=jnp.float32,
    )
    sq_ref[...] = square

    def q_copy(k):
        return remote(
            sq_ref, sq_got.at[k - 1], qs.at[k - 1], qr.at[k - 1], (me, lax.rem(mine + k, tps))
        )

    for k in range(1, tps):
        q_copy(k).start()

    def drain(s, carry):
        for d in (0, 1):
            m_copy(d, s).wait_send()
            for c in range(2):
                x_copy(d, s, c).wait_send()
            for c in range(cuts):
                copy(d, s, c).wait_send()
        return carry

    lax.fori_loop(0, n - 1, drain, 0)
    for k in range(1, tps):
        q_copy(k).wait()
    total = square
    for k in range(1, tps):
        total = total + sq_got[k - 1]
    scale = lax.rsqrt(total / (width * tps) + 1e-06)
    column = lax.dot_general(
        scale,
        jnp.full((8, LANES), 0.125, jnp.float32),
        (((0,), (0,)), ((), ())),
        precision=lax.Precision.HIGHEST,
        preferred_element_type=jnp.float32,
    )
    for c in range(width // LANES):
        at = slice(c * LANES, (c + 1) * LANES)
        out_ref[:, at] = (out_total[:, at] * column * gain_ref[:, at]).astype(jnp.bfloat16)


def body(tokens, row_ids, row_gates, key_table, value_table, norm_gain):
    block, width = tokens.shape
    picks = row_ids.shape[1]
    experts = key_table.shape[0]
    n, tps = lax.axis_size("ep"), lax.axis_size("tp")
    half = block // 2
    lines = half * picks // ROW
    cuts = 2 if width % (2 * LANES) == 0 else 1
    meta = jnp.concatenate(
        [
            row_ids.astype(jnp.float32).reshape(2, lines, ROW),
            row_gates.reshape(2, lines, ROW),
        ],
        axis=1,
    )
    whole = pl.BlockSpec(memory_space=pltpu.VMEM)
    hbm = pl.BlockSpec(memory_space=pl.ANY)
    dma = pltpu.SemaphoreType.DMA
    bf16, f32 = jnp.bfloat16, jnp.float32
    return pl.pallas_call(
        functools.partial(kernel, n, tps, picks, cycle_of(n)),
        out_shape=jax.ShapeDtypeStruct((block, width), bf16),
        in_specs=[whole, whole, hbm, hbm, whole],
        out_specs=whole,
        scratch_shapes=[
            pltpu.VMEM((experts, width), bf16),
            pltpu.VMEM((experts, width), bf16),
            pltpu.VMEM((n, block, width), bf16),
            pltpu.VMEM((n, 2, 2 * lines, ROW), f32),
            pltpu.VMEM((block, experts), f32),
            pltpu.VMEM((n, 2 * lines, ROW), f32),
            pltpu.VMEM((n, tps - 1, 2 * lines, ROW), f32),
            pltpu.VMEM((2 * lines, ROW), f32),
            pltpu.VMEM((block, experts), bf16),
            pltpu.VMEM((block, width), f32),
            pltpu.VMEM((n - 1, 2, cuts, half, width // cuts), bf16),
            pltpu.VMEM((n - 1, 2, cuts, half, width // cuts), bf16),
            pltpu.VMEM((8, block), f32),
            pltpu.VMEM((tps - 1, 8, block), f32),
            dma((2, n - 1, 2)),
            dma((2, n - 1, 2)),
            dma((2, n - 1)),
            dma((2, n - 1)),
            dma((n, tps - 1)),
            dma((n, tps - 1)),
            dma((2, n - 1, cuts)),
            dma((2, n - 1, cuts)),
            dma((tps - 1,)),
            dma((tps - 1,)),
            dma((2,)),
        ],
        compiler_params=pltpu.CompilerParams(collective_id=0, has_side_effects=True),
    )(tokens, meta, key_table, value_table, norm_gain.reshape(1, -1))


def solution(mesh):
    in_specs = (P("ep", "tp"), P("ep", None), P("ep", None), P("ep", "tp"), P("ep", "tp"), P("tp"))
    out_specs = P("ep", "tp")
    return jax.shard_map(body, mesh=mesh, in_specs=in_specs, out_specs=out_specs, check_vma=False)
```

profile of v0, /device:TPU:0, one launch (start us, length us, event | category | flops | bytes accessed | tf_op | source)
XLA Modules:
  0.0 75.1 jit_solution(12791510419693067018)
XLA Ops:
  0.0 0.7 convert_element_type.3
  0.7 0.1 copy.9
  0.8 0.1 reshape.9
  0.9 0.8 %copy.10 = f32[256,16]{1,0:T(8,128)S(1)} copy(f32[256,16]{0,1:T(8,128)} %param.8) | data formatting | bytes 32768 | tf_op args[2]
  1.8 0.1 reshape.10
  1.9 0.6 pad_maximum_fusion.refs_1_
  2.5 71.0 %shard_map.64 = bf16[256,512]{1,0:T(8,128)(2,1)} custom-call(bf16[256,512]{1,0:T(8,128)(2,1)} %refs_0_.1, f32[2,16,256]{2,1,0:T(8,128)} %pad_maximum_fusion.refs_1_, bf16[4096,512]{1,0:T(8,128)(2,1)} %refs_2_.1, bf16[4096,512]{1,0:T(8,128)(2,1)} %refs_3_.1, f32[1,512]{1,0:T(1,128)} %bitcast.1), custom_call_target="tpu_custom_call" | custom-call | tf_op jit(solution)/shard_map/pallas_call | solution.py:304
  73.5 1.7 %copy.12 = bf16[256,512]{1,0:T(8,128)(2,1)} copy(bf16[256,512]{1,0:T(8,128)(2,1)} %shard_map.64) | data formatting | bytes 524288
where the time goes:
time: 75.5 us; the launch traced here: 75.1 us
  Pallas kernels  71 us (94%)
  local copies, waits for them, and re-layouts  2.81 us (4%)
  other arithmetic  1.34 us (2%)
    pallas_call x1, Pallas kernels, body(): pl.pallas_call(functools.partial(kernel, n, tps, picks, cycle_of(n)), out...  71 us
    unnamed x2, local copies, waits for them, and re-layouts  2.49 us

commit v1 on v0

v1 whole, which is shorter than its diff:
```python
import functools

import jax
import jax.numpy as jnp
from jax import lax
from jax.experimental import pallas as pl
from jax.experimental.pallas import tpu as pltpu
from jax.sharding import PartitionSpec as P

ROW = 256
LANES = 128
MESH = pl.DeviceIdType.MESH


def cycle_of(n):
    x = 1
    while 4 * x * x <= n:
        x *= 2
    z = n // x
    if x == 1 or z % 2:
        return list(range(n))
    out = []
    for row in range(z):
        cols = range(1, x) if row % 2 == 0 else range(x - 1, 0, -1)
        out += [row * x + col for col in cols]
    return out + [row * x for row in range(z - 1, -1, -1)]


def look(table, i):
    n = len(table)
    total = 0
    for k, v in enumerate(table):
        total = total + v * ((n * n - (i - k) * (i - k)) // (n * n))
    return total


def greet(n, tps, me, order):
    pos = look([order.index(i) for i in range(n)], me)
    right = look(order, lax.rem(pos + 1, n))
    left = look(order, lax.rem(pos + n - 1, n))
    mine = lax.axis_index("tp")
    barrier = pltpu.get_barrier_semaphore()
    for peer in (left, right):
        pl.semaphore_signal(barrier, inc=1, device_id=(peer, mine), device_id_type=MESH)
    for k in range(1, tps):
        pl.semaphore_signal(
            barrier, inc=1, device_id=(me, lax.rem(mine + k, tps)), device_id_type=MESH
        )
    pl.semaphore_wait(barrier, 2 + tps - 1)
    return pos, right, left, mine


def remote(src, dst, send, recv, device):
    return pltpu.make_async_remote_copy(
        src_ref=src, dst_ref=dst, send_sem=send, recv_sem=recv, device_id=device, device_id_type=MESH
    )


def kernel(n, tps, picks, order, *refs):
    x_ref, meta_ref, key_hbm, value_hbm, gain_ref, out_ref = refs[:6]
    key_ref, value_ref, xall, metas, s_ref, part, got_ref, w_ref = refs[6:14]
    own, mix_ref, sent, came, sq_ref, sq_got = refs[14:20]
    xs, xr, ms, mr, ps, pr, ss, sr, qs, qr, kv = refs[20:]
    block, width = x_ref.shape
    half = block // 2
    experts = key_ref.shape[0]
    lines = meta_ref.shape[1] // 2
    cuts = xs.shape[2]
    rows = half // cuts
    key_copy = pltpu.make_async_copy(key_hbm, key_ref, kv.at[0])
    value_copy = pltpu.make_async_copy(value_hbm, value_ref, kv.at[1])
    key_copy.start()
    me = lax.axis_index("ep")
    pos, right, left, mine = greet(n, tps, me, order)
    base = me * experts
    peers = (right, left)

    def x_copy(d, step, c, first=False):
        at = pl.ds(d * half + c * rows, rows)
        src = x_ref.at[at] if first else xall.at[step, at]
        return remote(
            src, xall.at[step + 1, at], xs.at[d, step, c], xr.at[d, step, c], (peers[d], mine)
        )

    def m_copy(d, step, first=False):
        src = meta_ref.at[d] if first else metas.at[step, d]
        return remote(src, metas.at[step + 1, d], ms.at[d, step], mr.at[d, step], (peers[d], mine))

    def p_copy(s, k):
        return remote(
            part.at[s],
            got_ref.at[s, k - 1],
            ps.at[s, k - 1],
            pr.at[s, k - 1],
            (me, lax.rem(mine + k, tps)),
        )

    def r_copy(d, s, c):
        return remote(
            sent.at[s, d, c], came.at[s, d, c], ss.at[d, s, c], sr.at[d, s, c], (peers[d], mine)
        )

    for c in range(cuts):
        for d in (0, 1):
            x_copy(d, 0, c, True).start()
            if c == 0:
                m_copy(d, 0, True).start()
    xall[0] = x_ref[...]
    metas[0] = meta_ref[...]
    value_copy.start()
    key_copy.wait()

    per_half = LANES // picks
    sub = lax.broadcasted_iota(jnp.int32, (per_half, LANES), 0)
    lane = lax.broadcasted_iota(jnp.int32, (per_half, LANES), 1)
    own_lane = sub == lane // picks
    per = ROW // picks
    tall = experts // ROW * per
    lane_token = lax.broadcasted_iota(jnp.int32, (1, ROW), 1) // picks
    tall_iota = lax.broadcasted_iota(jnp.int32, (tall, ROW), 0)
    lo_iota = lax.broadcasted_iota(jnp.int32, (ROW, ROW), 0)
    spans = 2 * lines
    wide = experts // spans

    def gather_on(s, c):
        @pl.when(s < n)
        def _():
            for d in (0, 1):
                x_copy(d, s - 1, c).wait_recv()

                @pl.when(s < n - 1)
                def _():
                    x_copy(d, s, c).start()

                if c == 0:
                    m_copy(d, s - 1).wait_recv()

                    @pl.when(s < n - 1)
                    def _():
                        m_copy(d, s).start()

    def score(s, i):
        at = slice(i * wide, (i + 1) * wide)
        s_ref[:, at] = lax.dot_general(
            xall[s],
            key_ref[at, :],
            (((1,), (1,)), ((), ())),
            preferred_element_type=jnp.float32,
        )

    def choose(s, i):
        d, r = i // lines, i % lines
        for h2 in range(ROW // LANES):
            lanes = slice(h2 * LANES, (h2 + 1) * LANES)
            ids = metas[s, d, r : r + 1, lanes].astype(jnp.int32) - base
            ids = jnp.broadcast_to(ids, (per_half, LANES))
            owned = (ids >= 0) & (ids < experts)
            hi = jnp.where(owned, ids >> 7, -1)
            lo = jnp.where(owned, ids & (LANES - 1), 0)
            row = i * per + h2 * per_half
            acc = jnp.zeros((per_half, LANES), jnp.float32)
            for h in range(experts // LANES):
                tile = s_ref[row : row + per_half, h * LANES : (h + 1) * LANES]
                acc = jnp.where(hi == h, jnp.take_along_axis(tile, lo, axis=1), acc)
            part[s, i : i + 1, lanes] = jnp.sum(
                jnp.where(own_lane, acc, 0.0), axis=0, keepdims=True
            )

    def build(s, i):
        d, r = i // lines, i % lines
        total = part[s, i : i + 1, :]
        for k in range(1, tps):
            total = total + got_ref[s, k - 1, i : i + 1, :]
        h = 0.5 * total * (1.0 + lax.erf(total * (0.5**0.5))) * metas[s, d, lines + r : lines + r + 1, :]
        ids = metas[s, d, r : r + 1, :].astype(jnp.int32) - base
        owned = (ids >= 0) & (ids < experts)
        code = jnp.where(owned, (ids >> 8) * per + lane_token, -1)
        lo = ids & (ROW - 1)
        a = jnp.where(tall_iota == code, h, 0.0).astype(jnp.bfloat16)
        b = jnp.where(lo_iota == lo, 1.0, 0.0).astype(jnp.bfloat16)
        w = lax.dot_general(
            a, b, (((1,), (1,)), ((), ())), preferred_element_type=jnp.float32
        ).astype(jnp.bfloat16)
        for c in range(experts // ROW):
            w_ref[i * per : (i + 1) * per, c * ROW : (c + 1) * ROW] = w[c * per : (c + 1) * per, :]

    def send_part(s):
        for k in range(1, tps):
            p_copy(s, k).start()

    def wait_part(s):
        for k in range(1, tps):
            p_copy(s, k).wait()

    def blend(s, choosing):
        pieces = 4
        deep = experts // pieces
        mixed = None
        for q in range(pieces):
            at = slice(q * deep, (q + 1) * deep)
            dot = jnp.dot(w_ref[:, at], value_ref[at, :], preferred_element_type=jnp.float32)
            mixed = dot if mixed is None else mixed + dot
            if choosing is not None:
                for i in range(q * spans // pieces, (q + 1) * spans // pieces):
                    choose(choosing, i)
        mix_ref[...] = mixed

    def reduce_on(s, c):
        @pl.when((s >= 1) & (s < n))
        def _():
            for d in (0, 1):
                at = slice(d * half + c * rows, d * half + (c + 1) * rows)

                @pl.when(s >= 2)
                def _():
                    r_copy(d, s - 2, c).wait_recv()
                    sent[s - 1, d, c] = (
                        mix_ref[at, :] + came[s - 2, d, c].astype(jnp.float32)
                    ).astype(jnp.bfloat16)

                @pl.when(s == 1)
                def _():
                    sent[0, d, c] = mix_ref[at, :].astype(jnp.bfloat16)

                r_copy(d, s - 1, c).start()

    def keep(s):
        @pl.when(s == 0)
        def _():
            own[...] = mix_ref[...]

    def lead(t, carry):
        for i in range(spans):
            score(t, i)
        for i in range(spans):
            choose(t, i)
        send_part(t)
        for c in range(cuts):
            gather_on(t + 1, c)
        return carry

    lax.fori_loop(0, 2, lead, 0)
    value_copy.wait()
    first = cuts // 2

    def steady(t, carry):
        wait_part(t - 2)
        for i in range(spans):
            score(t, i)
            build(t - 2, i)
        for c in range(first):
            gather_on(t + 1, c)
        for c in range(first, cuts):
            reduce_on(t - 3, c)
        blend(t - 2, t)
        send_part(t)
        keep(t - 2)
        for c in range(first, cuts):
            gather_on(t + 1, c)
        for c in range(first):
            reduce_on(t - 2, c)
        return carry

    lax.fori_loop(2, n, steady, 0)

    def last(t, carry):
        wait_part(t - 2)
        for i in range(spans):
            build(t - 2, i)
        for c in range(first, cuts):
            reduce_on(t - 3, c)
        blend(t - 2, None)
        keep(t - 2)
        for c in range(first):
            reduce_on(t - 2, c)
        return carry

    lax.fori_loop(n, n + 2, last, 0)
    for c in range(first, cuts):
        reduce_on(n - 1, c)

    ones = jnp.ones((8, width), jnp.float32)
    for c in range(cuts):
        for d in (0, 1):
            at = slice(d * half + c * rows, d * half + (c + 1) * rows)
            r_copy(d, n - 2, c).wait_recv()
            own[at, :] = own[at, :] + came[n - 2, d, c].astype(jnp.float32)
    mixed = own[...]
    square = lax.dot_general(
        ones,
        mixed * mixed,
        (((1,), (1,)), ((), ())),
        precision=lax.Precision.HIGHEST,
        preferred_element_type=jnp.float32,
    )
    sq_ref[...] = square

    def q_copy(k):
        return remote(
            sq_ref, sq_got.at[k - 1], qs.at[k - 1], qr.at[k - 1], (me, lax.rem(mine + k, tps))
        )

    for k in range(1, tps):
        q_copy(k).start()

    def drain(s, carry):
        for d in (0, 1):
            m_copy(d, s).wait_send()
            for c in range(cuts):
                x_copy(d, s, c).wait_send()
                r_copy(d, s, c).wait_send()
        return carry

    lax.fori_loop(0, n - 1, drain, 0)
    for k in range(1, tps):
        q_copy(k).wait()
    total = square
    for k in range(1, tps):
        total = total + sq_got[k - 1]
    scale = lax.rsqrt(total / (width * tps) + 1e-06)
    column = lax.dot_general(
        scale,
        jnp.full((8, LANES), 0.125, jnp.float32),
        (((0,), (0,)), ((), ())),
        precision=lax.Precision.HIGHEST,
        preferred_element_type=jnp.float32,
    )
    for c in range(width // LANES):
        at = slice(c * LANES, (c + 1) * LANES)
        out_ref[:, at] = (own[:, at] * column * gain_ref[:, at]).astype(jnp.bfloat16)


def body(tokens, row_ids, row_gates, key_table, value_table, norm_gain):
    block, width = tokens.shape
    picks = row_ids.shape[1]
    experts = key_table.shape[0]
    n, tps = lax.axis_size("ep"), lax.axis_size("tp")
    half = block // 2
    lines = half * picks // ROW
    cuts = 2
    rows = half // cuts
    meta = jnp.concatenate(
        [
            row_ids.astype(jnp.float32).reshape(2, lines, ROW),
            row_gates.reshape(2, lines, ROW),
        ],
        axis=1,
    )
    whole = pl.BlockSpec(memory_space=pltpu.VMEM)
    hbm = pl.BlockSpec(memory_space=pl.ANY)
    dma = pltpu.SemaphoreType.DMA
    bf16, f32 = jnp.bfloat16, jnp.float32
    return pl.pallas_call(
        functools.partial(kernel, n, tps, picks, cycle_of(n)),
        out_shape=jax.ShapeDtypeStruct((block, width), bf16),
        in_specs=[whole, whole, hbm, hbm, whole],
        out_specs=whole,
        scratch_shapes=[
            pltpu.VMEM((experts, width), bf16),
            pltpu.VMEM((experts, width), bf16),
            pltpu.VMEM((n, block, width), bf16),
            pltpu.VMEM((n, 2, 2 * lines, ROW), f32),
            pltpu.VMEM((block, experts), f32),
            pltpu.VMEM((n, 2 * lines, ROW), f32),
            pltpu.VMEM((n, tps - 1, 2 * lines, ROW), f32),
            pltpu.VMEM((block, experts), bf16),
            pltpu.VMEM((block, width), f32),
            pltpu.VMEM((block, width), f32),
            pltpu.VMEM((n - 1, 2, cuts, rows, width), bf16),
            pltpu.VMEM((n - 1, 2, cuts, rows, width), bf16),
            pltpu.VMEM((8, block), f32),
            pltpu.VMEM((tps - 1, 8, block), f32),
            dma((2, n - 1, cuts)),
            dma((2, n - 1, cuts)),
            dma((2, n - 1)),
            dma((2, n - 1)),
            dma((n, tps - 1)),
            dma((n, tps - 1)),
            dma((2, n - 1, cuts)),
            dma((2, n - 1, cuts)),
            dma((tps - 1,)),
            dma((tps - 1,)),
            dma((2,)),
        ],
        compiler_params=pltpu.CompilerParams(collective_id=0, has_side_effects=True),
    )(tokens, meta, key_table, value_table, norm_gain.reshape(1, -1))


def solution(mesh):
    in_specs = (P("ep", "tp"), P("ep", None), P("ep", None), P("ep", "tp"), P("ep", "tp"), P("tp"))
    out_specs = P("ep", "tp")
    return jax.shard_map(body, mesh=mesh, in_specs=in_specs, out_specs=out_specs, check_vma=False)
```

time: 75.5 us -> 65.6 us (0.87)
  Pallas kernels: 71 us -> 61.1 us
    pallas_call x1, Pallas kernels: 71 us -> 61.1 us  [body(): pl.pallas_call(functools.partial(kernel, n, tps, picks, cycle_of(n)), out...]
where the time goes in v1:
time: 65.6 us; the launch traced here: 65.3 us
  Pallas kernels  61.1 us (93%)
  local copies, waits for them, and re-layouts  2.81 us (4%)
  other arithmetic  1.34 us (2%)
    pallas_call x1, Pallas kernels, body(): pl.pallas_call(functools.partial(kernel, n, tps, picks, cycle_of(n)), out...  61.1 us
    unnamed x2, local copies, waits for them, and re-layouts  2.49 us

profile of v1, /device:TPU:0, one launch (start us, length us, event | category | flops | bytes accessed | tf_op | source)
XLA Modules:
  0.0 65.3 jit_solution(1558340819751674387)
XLA Ops:
  0.0 0.7 %convert_element_type.3 = f32[256,16]{0,1:T(8,128)S(1)} convert(s32[256,16]{0,1:T(8,128)} %param.7) | non-fusion elementwise | flops 4096 | bytes 32768 | tf_op jit(solution)/shard_map/convert_element_type | solution.py:344
  0.7 0.1 copy.9
  0.8 0.1 reshape.9
  0.9 0.8 %copy.10 = f32[256,16]{1,0:T(8,128)S(1)} copy(f32[256,16]{0,1:T(8,128)} %param.8) | data formatting | bytes 32768 | tf_op args[2]
  1.8 0.1 reshape.10
  1.9 0.6 pad_maximum_fusion.refs_1_
  2.5 61.1 %shard_map.64 = bf16[256,512]{1,0:T(8,128)(2,1)} custom-call(bf16[256,512]{1,0:T(8,128)(2,1)} %refs_0_.1, f32[2,16,256]{2,1,0:T(8,128)} %pad_maximum_fusion.refs_1_, bf16[4096,512]{1,0:T(8,128)(2,1)} %refs_2_.1, bf16[4096,512]{1,0:T(8,128)(2,1)} %refs_3_.1, f32[1,512]{1,0:T(1,128)} %bitcast.1), custom_call_target="tpu_custom_call" | custom-call | tf_op jit(solution)/shard_map/pallas_call | solution.py:353
  63.6 1.7 %copy.12 = bf16[256,512]{1,0:T(8,128)(2,1)} copy(bf16[256,512]{1,0:T(8,128)(2,1)} %shard_map.64) | data formatting | bytes 524288

commit v2 on v1

v2 whole, which is shorter than its diff:
```python
import functools

import jax
import jax.numpy as jnp
from jax import lax
from jax.experimental import pallas as pl
from jax.experimental.pallas import tpu as pltpu
from jax.sharding import PartitionSpec as P

ROW = 256
LANES = 128
MESH = pl.DeviceIdType.MESH


def cycle_of(n):
    x = 1
    while 4 * x * x <= n:
        x *= 2
    z = n // x
    if x == 1 or z % 2:
        return list(range(n))
    out = []
    for row in range(z):
        cols = range(1, x) if row % 2 == 0 else range(x - 1, 0, -1)
        out += [row * x + col for col in cols]
    return out + [row * x for row in range(z - 1, -1, -1)]


def look(table, i):
    n = len(table)
    total = 0
    for k, v in enumerate(table):
        total = total + v * ((n * n - (i - k) * (i - k)) // (n * n))
    return total


def hello(n, tps, me, order):
    pos = look([order.index(i) for i in range(n)], me)
    right = look(order, lax.rem(pos + 1, n))
    left = look(order, lax.rem(pos + n - 1, n))
    mine = lax.axis_index("tp")
    barrier = pltpu.get_barrier_semaphore()
    for peer in (left, right):
        pl.semaphore_signal(barrier, inc=1, device_id=(peer, mine), device_id_type=MESH)
    for k in range(1, tps):
        pl.semaphore_signal(
            barrier, inc=1, device_id=(me, lax.rem(mine + k, tps)), device_id_type=MESH
        )
    return right, left, mine


def greeted(tps):
    pl.semaphore_wait(pltpu.get_barrier_semaphore(), 2 + tps - 1)


def remote(src, dst, send, recv, device):
    return pltpu.make_async_remote_copy(
        src_ref=src, dst_ref=dst, send_sem=send, recv_sem=recv, device_id=device, device_id_type=MESH
    )


def kernel(n, tps, picks, order, *refs):
    x_hbm, ids_hbm, gates_hbm, key_hbm, value_hbm, gain_hbm, out_ref = refs[:7]
    key_ref, value_ref, xall, metas, s_ref, part, got_ref, w_ref = refs[7:15]
    mix_ref, sent, came, sq_ref, sq_got = refs[15:20]
    ids_ref, gates_ref, gain_ref = refs[20:23]
    xr, mr, pr, sr, qr, ends, kv = refs[23:]
    cuts, rows, width = xall.shape[1], xall.shape[3], xall.shape[4]
    pair = 2 * rows
    block = cuts * pair
    half = block // 2
    experts = key_ref.shape[0]
    lines = metas.shape[2] // 2
    me = lax.axis_index("ep")
    right, left, mine = hello(n, tps, me, order)
    ids_copy = pltpu.make_async_copy(ids_hbm, ids_ref, kv.at[0])
    gates_copy = pltpu.make_async_copy(gates_hbm, gates_ref, kv.at[1])
    key_copy = pltpu.make_async_copy(key_hbm, key_ref, kv.at[3])
    value_copy = pltpu.make_async_copy(value_hbm, value_ref, kv.at[4])
    gain_copy = pltpu.make_async_copy(gain_hbm, gain_ref, kv.at[5])
    ids_copy.start()
    gates_copy.start()
    for c in range(cuts):
        for d in (0, 1):
            pltpu.make_async_copy(
                x_hbm.at[pl.ds(d * half + c * rows, rows)], xall.at[0, c, d], kv.at[2]
            ).start()
    for copy in (key_copy, value_copy, gain_copy):
        copy.start()
    base = me * experts
    peers = (right, left)
    near = n // 2 + n // 8
    far = n - 1 - near

    def x_copy(d, step, c):
        return remote(
            xall.at[step, c, d],
            xall.at[step + 1, c, d],
            ends.at[0],
            xr.at[step, c],
            (peers[d], mine),
        )

    def m_copy(d, step):
        return remote(
            metas.at[step, d], metas.at[step + 1, d], ends.at[1], mr.at[step], (peers[d], mine)
        )

    def far_copy(d, hop, c):
        return remote(
            xall.at[lax.rem(n - hop, n), c, 1 - d],
            xall.at[n - 1 - hop, c, 1 - d],
            ends.at[0],
            xr.at[near + hop, c],
            (peers[d], mine),
        )

    def far_meta(d, hop):
        return remote(
            metas.at[lax.rem(n - hop, n), 1 - d],
            metas.at[n - 1 - hop, 1 - d],
            ends.at[1],
            mr.at[near + hop],
            (peers[d], mine),
        )

    def p_copy(s, k):
        return remote(
            part.at[s],
            got_ref.at[s, k - 1],
            ends.at[2],
            pr.at[s],
            (me, lax.rem(mine + k, tps)),
        )

    def r_copy(d, s, c):
        return remote(
            sent.at[s, c, d], came.at[s, c, d], ends.at[3], sr.at[s, c], (peers[d], mine)
        )

    def arrived(ref, sem):
        pltpu.make_async_copy(ref, ref, sem).wait()

    per_half = LANES // picks
    per = ROW // picks
    pick_row = lax.broadcasted_iota(jnp.int32, (picks, LANES), 0)
    pick_lane = lax.broadcasted_iota(jnp.int32, (picks, LANES), 1) // per_half
    ids_copy.wait()
    gates_copy.wait()
    for which, table in enumerate((ids_ref[...].astype(jnp.float32), gates_ref[...])):
        for tile in range(block // LANES):
            slanted = pltpu.roll(
                table[:, tile * LANES : (tile + 1) * LANES], 0, 1, stride=per_half, stride_axis=0
            )
            for g in range(picks):
                moved = pltpu.roll(slanted, (LANES - g * per_half) % LANES, 1) if g else slanted
                line = jnp.sum(
                    jnp.where(pick_row == pick_lane, moved, 0.0), axis=0, keepdims=True
                )
                i, h2 = divmod(tile * picks + g, 2)
                d, r = divmod(i, lines)
                metas[
                    0, d, which * lines + r : which * lines + r + 1, h2 * LANES : (h2 + 1) * LANES
                ] = line
    arrived(xall.at[0], kv.at[2])
    greeted(tps)
    for c in range(cuts):
        for d in (0, 1):
            x_copy(d, 0, c).start()
            if c == 0:
                m_copy(d, 0).start()

    sub = lax.broadcasted_iota(jnp.int32, (per_half, LANES), 0)
    lane = lax.broadcasted_iota(jnp.int32, (per_half, LANES), 1)
    own_lane = sub == lane % per_half
    tall = experts // ROW * per
    flat = lax.broadcasted_iota(jnp.int32, (1, ROW), 1)
    lane_token = flat // LANES * per_half + flat % per_half
    tall_iota = lax.broadcasted_iota(jnp.int32, (tall, ROW), 0)
    lo_iota = lax.broadcasted_iota(jnp.int32, (ROW, ROW), 0)
    spans = 2 * lines
    wide = experts // spans
    each = rows // per

    def place(i):
        return i // each % 2, i // (2 * each) * each + i % each

    def gather_on(s, c):
        @pl.when(s <= near)
        def _():
            arrived(xall.at[s, c], xr.at[s - 1, c])

            @pl.when(s < near)
            def _():
                for d in (0, 1):
                    x_copy(d, s, c).start()

            if c == 0:
                arrived(metas.at[s], mr.at[s - 1])

                @pl.when(s < near)
                def _():
                    for d in (0, 1):
                        m_copy(d, s).start()

    items = (far + 1) * cuts if far else 0

    def far_on(f):
        hop, c = f // cuts, f % cuts

        @pl.when(f < items)
        def _():
            @pl.when(hop > 0)
            def _():
                arrived(xall.at[n - hop, c], xr.at[near + hop - 1, c])

            @pl.when(hop < far)
            def _():
                for d in (0, 1):
                    far_copy(d, hop, c).start()

            @pl.when(c == 0)
            def _():
                @pl.when(hop > 0)
                def _():
                    arrived(metas.at[n - hop], mr.at[near + hop - 1])

                @pl.when(hop < far)
                def _():
                    for d in (0, 1):
                        far_meta(d, hop).start()

    def far_step(t, c):
        done = 2 * near - 2
        rest = -(-(items - done) // cuts)
        if c % 2:

            @pl.when(t < near)
            def _():
                far_on(2 * t - 2 + c // 2)

        @pl.when(t == near)
        def _():
            for f in range(done + c * rest, done + (c + 1) * rest):
                far_on(f)

    def score(s, i):
        at = slice(i * wide, (i + 1) * wide)
        s_ref[:, at] = lax.dot_general(
            xall[s].reshape(block, width),
            key_ref[at, :],
            (((1,), (1,)), ((), ())),
            preferred_element_type=jnp.float32,
        )

    def choose(s, i):
        d, r = place(i)
        for h2 in range(ROW // LANES):
            lanes = slice(h2 * LANES, (h2 + 1) * LANES)
            ids = metas[s, d, r : r + 1, lanes].astype(jnp.int32) - base
            ids = jnp.broadcast_to(ids, (per_half, LANES))
            owned = (ids >= 0) & (ids < experts)
            hi = jnp.where(owned, ids >> 7, -1)
            lo = jnp.where(owned, ids & (LANES - 1), 0)
            row = i * per + h2 * per_half
            acc = jnp.zeros((per_half, LANES), jnp.float32)
            for h in range(experts // LANES):
                tile = s_ref[row : row + per_half, h * LANES : (h + 1) * LANES]
                acc = jnp.where(hi == h, jnp.take_along_axis(tile, lo, axis=1), acc)
            part[s, i : i + 1, lanes] = jnp.sum(
                jnp.where(own_lane, acc, 0.0), axis=0, keepdims=True
            )

    def build(s, i):
        d, r = place(i)
        total = part[s, i : i + 1, :]
        for k in range(1, tps):
            total = total + got_ref[s, k - 1, i : i + 1, :]
        gate = metas[s, d, lines + r : lines + r + 1, :]
        h = 0.5 * total * (1.0 + lax.erf(total * (0.5**0.5))) * gate
        ids = metas[s, d, r : r + 1, :].astype(jnp.int32) - base
        owned = (ids >= 0) & (ids < experts)
        code = jnp.where(owned, (ids >> 8) * per + lane_token, -1)
        lo = ids & (ROW - 1)
        a = jnp.where(tall_iota == code, h, 0.0).astype(jnp.bfloat16)
        b = jnp.where(lo_iota == lo, 1.0, 0.0).astype(jnp.bfloat16)
        w = lax.dot_general(
            a, b, (((1,), (1,)), ((), ())), preferred_element_type=jnp.float32
        ).astype(jnp.bfloat16)
        for c in range(experts // ROW):
            w_ref[i * per : (i + 1) * per, c * ROW : (c + 1) * ROW] = w[c * per : (c + 1) * per, :]

    def send_part(s):
        for k in range(1, tps):
            p_copy(s, k).start()

    def wait_part(s):
        arrived(got_ref.at[s], pr.at[s])

    def blend(s, q, choosing):
        pieces = 2
        deep = experts // (2 * pieces)
        mixed = None
        for p in range(pieces):
            at = slice((q * pieces + p) * deep, (q * pieces + p + 1) * deep)
            dot = jnp.dot(w_ref[:, at], value_ref[at, :], preferred_element_type=jnp.float32)
            mixed = dot if mixed is None else mixed + dot
            if choosing is not None:
                count = spans // (2 * pieces)
                for i in range((q * pieces + p) * count, (q * pieces + p + 1) * count):
                    choose(choosing, i)
        slot = lax.rem(s, 2)
        mix_ref[slot] = mixed if q == 0 else mix_ref[slot] + mixed

    def reduce_on(s, c):
        @pl.when((s >= 1) & (s < n))
        def _():
            at = slice(c * pair, (c + 1) * pair)
            share = mix_ref.at[lax.rem(s, 2)]

            @pl.when(s >= 2)
            def _():
                arrived(came.at[s - 2, c], sr.at[s - 2, c])
                before = came[s - 2, c].reshape(pair, width).astype(jnp.float32)
                sent[s - 1, c] = (share[at, :] + before).astype(jnp.bfloat16).reshape(2, rows, width)

            @pl.when(s == 1)
            def _():
                sent[0, c] = share[at, :].astype(jnp.bfloat16).reshape(2, rows, width)

            for d in (0, 1):
                r_copy(d, s - 1, c).start()

    key_copy.wait()
    far_on(0)
    for i in range(spans):
        score(0, i)
    for i in range(spans):
        choose(0, i)
    send_part(0)
    for c in range(cuts):
        gather_on(1, c)
    far_on(1)

    def lead(t, carry):
        for i in range(spans):
            score(t, i)
        for c in range(cuts // 2):
            gather_on(t + 1, c)

            @pl.when(t > 1)
            def _():
                far_step(t, c)

        for i in range(spans):
            choose(t, i)
        send_part(t)
        for c in range(cuts // 2, cuts):
            gather_on(t + 1, c)

            @pl.when(t > 1)
            def _():
                far_step(t, c)

        return carry

    lax.fori_loop(1, 3, lead, 0)
    value_copy.wait()

    def steady(t, carry):
        wait_part(t - 2)
        for q in (0, 1):
            for i in range(q * spans // 2, (q + 1) * spans // 2):
                score(t, i)
                build(t - 2, i)
            gather_on(t + 1, q)
            far_step(t, q)
            reduce_on(t - 3, 1 + q)
        blend(t - 2, 0, t)
        gather_on(t + 1, 2)
        far_step(t, 2)
        reduce_on(t - 3, 3)
        blend(t - 2, 1, t)
        send_part(t)
        gather_on(t + 1, 3)
        far_step(t, 3)
        reduce_on(t - 2, 0)
        return carry

    lax.fori_loop(3, n, steady, 0)

    def last(t, carry):
        slot = lax.rem(t - 2, n)
        wait_part(slot)
        for q in (0, 1):
            for i in range(q * spans // 2, (q + 1) * spans // 2):
                build(slot, i)
            reduce_on(t - 3, 1 + q)
        blend(slot, 0, None)
        reduce_on(t - 3, 3)
        blend(slot, 1, None)
        reduce_on(t - 2, 0)
        return carry

    lax.fori_loop(n, n + 3, last, 0)

    gain_copy.wait()
    places = lax.broadcasted_iota(jnp.int32, (8, LANES), 1)
    squares = jnp.zeros((8, LANES), jnp.float32)
    for c in range(cuts):
        arrived(came.at[n - 2, c], sr.at[n - 2, c])
        at = slice(c * pair, (c + 1) * pair)
        mixed = mix_ref[0, at, :] + came[n - 2, c].reshape(pair, width).astype(jnp.float32)
        mix_ref[0, at, :] = mixed
        folded = sum(
            mixed[:, k : k + LANES] * mixed[:, k : k + LANES] for k in range(0, width, LANES)
        )
        for g in range(pair // 8):
            line = jnp.sum(folded[g * 8 : (g + 1) * 8, :], axis=1, keepdims=True)
            squares = jnp.where(places == c * (pair // 8) + g, line, squares)
    sq_ref[...] = squares
    for k in range(1, tps):
        remote(
            sq_ref, sq_got.at[k - 1], ends.at[4], qr.at[0], (me, lax.rem(mine + k, tps))
        ).start()
    arrived(xall.at[pl.ds(1, n - 1)], ends.at[0])
    arrived(metas.at[pl.ds(1, n - 1)], ends.at[1])
    arrived(got_ref, ends.at[2])
    arrived(sent, ends.at[3])
    arrived(sq_got, qr.at[0])
    total = squares
    for k in range(1, tps):
        total = total + sq_got[k - 1]
    scale = lax.rsqrt(total / (width * tps) + 1e-06)
    gain = gain_ref[...]
    for g in range(0, block // 8, 2):
        column = jnp.concatenate([scale[:, g : g + 1], scale[:, g + 1 : g + 2]], axis=0)
        c, within = divmod(g * 8, pair)
        d, r = divmod(within, rows)
        token = d * half + c * rows + r
        out_ref[token : token + 16, :] = (
            mix_ref[0, g * 8 : g * 8 + 16, :] * column * gain
        ).astype(jnp.bfloat16)
    arrived(sq_got, ends.at[4])


def body(tokens, row_ids, row_gates, key_table, value_table, norm_gain):
    block, width = tokens.shape
    picks = row_ids.shape[1]
    experts = key_table.shape[0]
    n, tps = lax.axis_size("ep"), lax.axis_size("tp")
    half = block // 2
    lines = half * picks // ROW
    cuts = 4
    rows = half // cuts
    whole = pl.BlockSpec(memory_space=pltpu.VMEM)
    hbm = pl.BlockSpec(memory_space=pl.ANY)
    dma = pltpu.SemaphoreType.DMA
    bf16, f32 = jnp.bfloat16, jnp.float32
    return pl.pallas_call(
        functools.partial(kernel, n, tps, picks, cycle_of(n)),
        out_shape=pltpu.VMEM((block, width), bf16),
        in_specs=[hbm] * 6,
        out_specs=whole,
        scratch_shapes=[
            pltpu.VMEM((experts, width), bf16),
            pltpu.VMEM((experts, width), bf16),
            pltpu.VMEM((n, cuts, 2, rows, width), bf16),
            pltpu.VMEM((n, 2, 2 * lines, ROW), f32),
            pltpu.VMEM((block, experts), f32),
            pltpu.VMEM((n, 2 * lines, ROW), f32),
            pltpu.VMEM((n, tps - 1, 2 * lines, ROW), f32),
            pltpu.VMEM((block, experts), bf16),
            pltpu.VMEM((2, block, width), f32),
            pltpu.VMEM((n - 1, cuts, 2, rows, width), bf16),
            pltpu.VMEM((n - 1, cuts, 2, rows, width), bf16),
            pltpu.VMEM((8, LANES), f32),
            pltpu.VMEM((tps - 1, 8, LANES), f32),
            pltpu.VMEM((picks, block), jnp.int32),
            pltpu.VMEM((picks, block), f32),
            pltpu.VMEM((1, width), f32),
            dma((n - 1, cuts)),
            dma((n - 1,)),
            dma((n,)),
            dma((n - 1, cuts)),
            dma((1,)),
            dma((5,)),
            dma((6,)),
        ],
        compiler_params=pltpu.CompilerParams(collective_id=0, has_side_effects=True),
    )(tokens, row_ids.T, row_gates.T, key_table, value_table, norm_gain.reshape(1, -1))


def solution(mesh):
    in_specs = (P("ep", "tp"), P("ep", None), P("ep", None), P("ep", "tp"), P("ep", "tp"), P("tp"))
    out_specs = P("ep", "tp")
    return jax.shard_map(body, mesh=mesh, in_specs=in_specs, out_specs=out_specs, check_vma=False)
```

time: 65.6 us -> 57.2 us (0.87)
  Pallas kernels: 61.1 us -> 56.3 us
  local copies, waits for them, and re-layouts: 2.81 us -> 0.71 us
  other arithmetic: 1.34 us -> 0 us
    pallas_call x1, Pallas kernels: 61.1 us -> 56.3 us  [body(): pl.pallas_call(functools.partial(kernel, n, tps, picks, cycle_of(n)), out...]
    unnamed x2 -> x1, local copies, waits for them, and re-layouts: 2.49 us -> 0.71 us
    convert_element_type x1 -> x0, other arithmetic: 0.72 us -> none  [body(): row_ids.astype(jnp.float32).reshape(2, lines, ROW)]
where the time goes in v2:
time: 57.2 us; the launch traced here: 57 us
  Pallas kernels  56.3 us (98%)
  local copies, waits for them, and re-layouts  0.71 us (1%)
    pallas_call x1, Pallas kernels, body(): pl.pallas_call(functools.partial(kernel, n, tps, picks, cycle_of(n)), out...  56.3 us

profile of v2, /device:TPU:0, one launch (start us, length us, event | category | flops | bytes accessed | tf_op | source)
XLA Modules:
  0.0 57.0 jit_solution(13316302201679145129)
XLA Ops:
  0.0 56.3 %shard_map.64 = bf16[256,512]{1,0:T(8,128)(2,1)S(1)} custom-call(bf16[256,512]{1,0:T(8,128)(2,1)} %refs_0_.1, s32[16,256]{1,0:T(8,128)} %bitcast.3, f32[16,256]{1,0:T(8,128)} %bitcast.4, bf16[4096,512]{1,0:T(8,128)(2,1)} %refs_3_.1, bf16[4096,512]{1,0:T(8,128)(2,1)} %refs_4_.1, f32[1,512]{1,0:T(1,128)} %bitcast.5), custom_call_target="tpu_custom_call" | custom-call | tf_op jit(solution)/shard_map/pallas_call | solution.py:460
  56.3 0.7 %copy.8 = bf16[256,512]{1,0:T(8,128)(2,1)} copy(bf16[256,512]{1,0:T(8,128)(2,1)S(1)} %shard_map.64) | data formatting | bytes 524288

commit v3 on v2

--- a/solution.py
+++ b/solution.py
@@ -89,8 +89,7 @@
         copy.start()
     base = me * experts
     peers = (right, left)
-    near = n // 2 + n // 8
-    far = n - 1 - near
+    near = n - 2
 
     def x_copy(d, step, c):
         return remote(
@@ -106,22 +105,14 @@
             metas.at[step, d], metas.at[step + 1, d], ends.at[1], mr.at[step], (peers[d], mine)
         )
 
-    def far_copy(d, hop, c):
-        return remote(
-            xall.at[lax.rem(n - hop, n), c, 1 - d],
-            xall.at[n - 1 - hop, c, 1 - d],
-            ends.at[0],
-            xr.at[near + hop, c],
-            (peers[d], mine),
-        )
-
-    def far_meta(d, hop):
-        return remote(
-            metas.at[lax.rem(n - hop, n), 1 - d],
-            metas.at[n - 1 - hop, 1 - d],
-            ends.at[1],
-            mr.at[near + hop],
-            (peers[d], mine),
+    def far_copy(d, c):
+        return remote(
+            xall.at[0, c, 1 - d], xall.at[n - 1, c, 1 - d], ends.at[0], xr.at[near, c], (peers[d], mine)
+        )
+
+    def far_meta(d):
+        return remote(
+            metas.at[0, 1 - d], metas.at[n - 1, 1 - d], ends.at[1], mr.at[near], (peers[d], mine)
         )
 
     def p_copy(s, k):
@@ -203,46 +194,16 @@
                     for d in (0, 1):
                         m_copy(d, s).start()
 
-    items = (far + 1) * cuts if far else 0
-
-    def far_on(f):
-        hop, c = f // cuts, f % cuts
-
-        @pl.when(f < items)
-        def _():
-            @pl.when(hop > 0)
-            def _():
-                arrived(xall.at[n - hop, c], xr.at[near + hop - 1, c])
-
-            @pl.when(hop < far)
-            def _():
-                for d in (0, 1):
-                    far_copy(d, hop, c).start()
-
-            @pl.when(c == 0)
-            def _():
-                @pl.when(hop > 0)
-                def _():
-                    arrived(metas.at[n - hop], mr.at[near + hop - 1])
-
-                @pl.when(hop < far)
-                def _():
-                    for d in (0, 1):
-                        far_meta(d, hop).start()
-
-    def far_step(t, c):
-        done = 2 * near - 2
-        rest = -(-(items - done) // cuts)
-        if c % 2:
-
-            @pl.when(t < near)
-            def _():
-                far_on(2 * t - 2 + c // 2)
-
-        @pl.when(t == near)
-        def _():
-            for f in range(done + c * rest, done + (c + 1) * rest):
-                far_on(f)
+    def far_start(c):
+        for d in (0, 1):
+            far_copy(d, c).start()
+            if c == 0:
+                far_meta(d).start()
+
+    def far_end():
+        arrived(metas.at[n - 1], mr.at[near])
+        for c in range(cuts):
+            arrived(xall.at[n - 1, c], xr.at[near, c])
 
     def score(s, i):
         at = slice(i * wide, (i + 1) * wide)
@@ -313,26 +274,28 @@
         mix_ref[slot] = mixed if q == 0 else mix_ref[slot] + mixed
 
     def reduce_on(s, c):
-        @pl.when((s >= 1) & (s < n))
+        @pl.when(s == 1)
         def _():
             at = slice(c * pair, (c + 1) * pair)
-            share = mix_ref.at[lax.rem(s, 2)]
-
-            @pl.when(s >= 2)
-            def _():
-                arrived(came.at[s - 2, c], sr.at[s - 2, c])
-                before = came[s - 2, c].reshape(pair, width).astype(jnp.float32)
-                sent[s - 1, c] = (share[at, :] + before).astype(jnp.bfloat16).reshape(2, rows, width)
-
-            @pl.when(s == 1)
-            def _():
-                sent[0, c] = share[at, :].astype(jnp.bfloat16).reshape(2, rows, width)
-
+            sent[0, c] = mix_ref[1, at, :].astype(jnp.bfloat16).reshape(2, rows, width)
             for d in (0, 1):
-                r_copy(d, s - 1, c).start()
+                r_copy(d, 0, c).start()
+
+        @pl.when(s >= 2)
+        def _():
+            pass_sum(s, c)
+
+    def pass_sum(s, c):
+        at = slice(c * pair, (c + 1) * pair)
+        arrived(came.at[s - 2, c], sr.at[s - 2, c])
+        before = came[s - 2, c].reshape(pair, width).astype(jnp.float32)
+        share = mix_ref[lax.rem(s, 2), at, :]
+        sent[s - 1, c] = (share + before).astype(jnp.bfloat16).reshape(2, rows, width)
+        for d in (0, 1):
+            r_copy(d, s - 1, c).start()
 
     key_copy.wait()
-    far_on(0)
+    far_start(0)
     for i in range(spans):
         score(0, i)
     for i in range(spans):
@@ -340,28 +303,18 @@
     send_part(0)
     for c in range(cuts):
         gather_on(1, c)
-    far_on(1)
 
     def lead(t, carry):
-        for i in range(spans):
-            score(t, i)
-        for c in range(cuts // 2):
-            gather_on(t + 1, c)
-
-            @pl.when(t > 1)
-            def _():
-                far_step(t, c)
-
-        for i in range(spans):
-            choose(t, i)
-        send_part(t)
-        for c in range(cuts // 2, cuts):
-            gather_on(t + 1, c)
-
-            @pl.when(t > 1)
-            def _():
-                far_step(t, c)
-
+        for q in range(cuts):
+            part_of = spans * 2 // cuts
+            for i in range(q * part_of, (q + 1) * part_of):
+                if i < spans:
+                    score(t, i)
+                else:
+                    choose(t, i - spans)
+            if q == cuts - 1:
+                send_part(t)
+            gather_on(t + 1, q)
         return carry
 
     lax.fori_loop(1, 3, lead, 0)
@@ -374,35 +327,76 @@
                 score(t, i)
                 build(t - 2, i)
             gather_on(t + 1, q)
-            far_step(t, q)
+            if q == 1:
+
+                @pl.when(t == 3)
+                def _():
+                    far_start(1)
+
             reduce_on(t - 3, 1 + q)
         blend(t - 2, 0, t)
         gather_on(t + 1, 2)
-        far_step(t, 2)
+
+        @pl.when(t == near - 1)
+        def _():
+            far_start(2)
+
         reduce_on(t - 3, 3)
         blend(t - 2, 1, t)
         send_part(t)
         gather_on(t + 1, 3)
-        far_step(t, 3)
         reduce_on(t - 2, 0)
+
+        @pl.when(t == near - 1)
+        def _():
+            far_start(3)
+
         return carry
 
-    lax.fori_loop(3, n, steady, 0)
-
-    def last(t, carry):
-        slot = lax.rem(t - 2, n)
-        wait_part(slot)
+    lax.fori_loop(3, near, steady, 0)
+
+    def late(t, carry):
+        wait_part(t - 2)
         for q in (0, 1):
             for i in range(q * spans // 2, (q + 1) * spans // 2):
-                build(slot, i)
-            reduce_on(t - 3, 1 + q)
-        blend(slot, 0, None)
-        reduce_on(t - 3, 3)
-        blend(slot, 1, None)
-        reduce_on(t - 2, 0)
+                score(t, i)
+                build(t - 2, i)
+            pass_sum(t - 3, 1 + q)
+        blend(t - 2, 0, t)
+        pass_sum(t - 3, 3)
+        blend(t - 2, 1, t)
+        send_part(t)
+        pass_sum(t - 2, 0)
+
+        @pl.when(t == near)
+        def _():
+            far_end()
+
         return carry
 
-    lax.fori_loop(n, n + 3, last, 0)
+    lax.fori_loop(near, n, late, 0)
+
+    def last(t, carry):
+        wait_part(t - 2)
+        for q in (0, 1):
+            for i in range(q * spans // 2, (q + 1) * spans // 2):
+                build(t - 2, i)
+            pass_sum(t - 3, 1 + q)
+        blend(t - 2, 0, None)
+        pass_sum(t - 3, 3)
+        blend(t - 2, 1, None)
+        pass_sum(t - 2, 0)
+        return carry
+
+    lax.fori_loop(n, n + 2, last, 0)
+    wait_part(0)
+    for q in (0, 1):
+        for i in range(q * spans // 2, (q + 1) * spans // 2):
+            build(0, i)
+        pass_sum(n - 1, 1 + q)
+    blend(0, 0, None)
+    pass_sum(n - 1, 3)
+    blend(0, 1, None)
 
     gain_copy.wait()
     places = lax.broadcasted_iota(jnp.int32, (8, LANES), 1)

time: 57.2 us -> 56 us (0.979)
  Pallas kernels: 56.3 us -> 55 us
    pallas_call x1, Pallas kernels: 56.3 us -> 55 us  [body(): pl.pallas_call(functools.partial(kernel, n, tps, picks, cycle_of(n)), out...]
where the time goes in v3:
time: 56 us; the launch traced here: 55.7 us
  Pallas kernels  55 us (98%)
  local copies, waits for them, and re-layouts  0.71 us (1%)
    pallas_call x1, Pallas kernels, body(): pl.pallas_call(functools.partial(kernel, n, tps, picks, cycle_of(n)), out...  55 us

profile of v3, /device:TPU:0, one launch (start us, length us, event | category | flops | bytes accessed | tf_op | source)
XLA Modules:
  0.0 55.7 jit_solution(14557964456094675812)
XLA Ops:
  0.0 55.0 %shard_map.64 = bf16[256,512]{1,0:T(8,128)(2,1)S(1)} custom-call(bf16[256,512]{1,0:T(8,128)(2,1)} %refs_0_.1, s32[16,256]{1,0:T(8,128)} %bitcast.3, f32[16,256]{1,0:T(8,128)} %bitcast.4, bf16[4096,512]{1,0:T(8,128)(2,1)} %refs_3_.1, bf16[4096,512]{1,0:T(8,128)(2,1)} %refs_4_.1, f32[1,512]{1,0:T(1,128)} %bitcast.5), custom_call_target="tpu_custom_call" | custom-call | tf_op jit(solution)/shard_map/pallas_call | solution.py:454
  55.0 0.7 %copy.8 = bf16[256,512]{1,0:T(8,128)(2,1)} copy(bf16[256,512]{1,0:T(8,128)(2,1)S(1)} %shard_map.64) | data formatting | bytes 524288

commit v4 on v3

--- a/solution.py
+++ b/solution.py
@@ -64,13 +64,14 @@
     key_ref, value_ref, xall, metas, s_ref, part, got_ref, w_ref = refs[7:15]
     mix_ref, sent, came, sq_ref, sq_got = refs[15:20]
     ids_ref, gates_ref, gain_ref = refs[20:23]
-    xr, mr, pr, sr, qr, ends, kv = refs[23:]
+    xr, mr, tr, pr, sr, qr, ends, kv = refs[23:]
     cuts, rows, width = xall.shape[1], xall.shape[3], xall.shape[4]
     pair = 2 * rows
     block = cuts * pair
     half = block // 2
     experts = key_ref.shape[0]
-    lines = metas.shape[2] // 2
+    group = metas.shape[3]
+    lines = group * metas.shape[1] // 2
     me = lax.axis_index("ep")
     right, left, mine = hello(n, tps, me, order)
     ids_copy = pltpu.make_async_copy(ids_hbm, ids_ref, kv.at[0])
@@ -96,23 +97,44 @@
             xall.at[step, c, d],
             xall.at[step + 1, c, d],
             ends.at[0],
-            xr.at[step, c],
+            xr.at[lax.rem(step, 2), c],
             (peers[d], mine),
         )
 
     def m_copy(d, step):
         return remote(
-            metas.at[step, d], metas.at[step + 1, d], ends.at[1], mr.at[step], (peers[d], mine)
-        )
+            metas.at[step, mine, d],
+            metas.at[step + 1, mine, d],
+            ends.at[1],
+            mr.at[lax.rem(step, 2)],
+            (peers[d], mine),
+        )
+
+    def share_meta(s):
+        for k in range(1, tps):
+            remote(
+                metas.at[s, mine],
+                metas.at[s, mine],
+                ends.at[5],
+                tr.at[s - 1],
+                (me, lax.rem(mine + k, tps)),
+            ).start()
+
+    def wait_meta(s):
+        arrived(metas.at[s, pl.ds(0, tps - 1)], tr.at[s - 1])
 
     def far_copy(d, c):
         return remote(
-            xall.at[0, c, 1 - d], xall.at[n - 1, c, 1 - d], ends.at[0], xr.at[near, c], (peers[d], mine)
+            xall.at[0, c, 1 - d], xall.at[n - 1, c, 1 - d], ends.at[0], xr.at[2, c], (peers[d], mine)
         )
 
     def far_meta(d):
         return remote(
-            metas.at[0, 1 - d], metas.at[n - 1, 1 - d], ends.at[1], mr.at[near], (peers[d], mine)
+            metas.at[0, mine, 1 - d],
+            metas.at[n - 1, mine, 1 - d],
+            ends.at[1],
+            mr.at[2],
+            (peers[d], mine),
         )
 
     def p_copy(s, k):
@@ -126,7 +148,7 @@
 
     def r_copy(d, s, c):
         return remote(
-            sent.at[s, c, d], came.at[s, c, d], ends.at[3], sr.at[s, c], (peers[d], mine)
+            sent.at[s, c, d], came.at[s, c, d], ends.at[3], sr.at[lax.rem(s, 2), c], (peers[d], mine)
         )
 
     def arrived(ref, sem):
@@ -136,6 +158,11 @@
     per = ROW // picks
     pick_row = lax.broadcasted_iota(jnp.int32, (picks, LANES), 0)
     pick_lane = lax.broadcasted_iota(jnp.int32, (picks, LANES), 1) // per_half
+    arrived(xall.at[0], kv.at[2])
+    greeted(tps)
+    for c in range(cuts // 2):
+        for d in (0, 1):
+            x_copy(d, 0, c).start()
     ids_copy.wait()
     gates_copy.wait()
     for which, table in enumerate((ids_ref[...].astype(jnp.float32), gates_ref[...])):
@@ -150,16 +177,13 @@
                 )
                 i, h2 = divmod(tile * picks + g, 2)
                 d, r = divmod(i, lines)
-                metas[
-                    0, d, which * lines + r : which * lines + r + 1, h2 * LANES : (h2 + 1) * LANES
-                ] = line
-    arrived(xall.at[0], kv.at[2])
-    greeted(tps)
-    for c in range(cuts):
+                q, r = divmod(which * lines + r, group)
+                metas[0, q, d, r : r + 1, h2 * LANES : (h2 + 1) * LANES] = line
+    for d in (0, 1):
+        m_copy(d, 0).start()
+    for c in range(cuts // 2, cuts):
         for d in (0, 1):
             x_copy(d, 0, c).start()
-            if c == 0:
-                m_copy(d, 0).start()
 
     sub = lax.broadcasted_iota(jnp.int32, (per_half, LANES), 0)
     lane = lax.broadcasted_iota(jnp.int32, (per_half, LANES), 1)
@@ -176,10 +200,13 @@
     def place(i):
         return i // each % 2, i // (2 * each) * each + i % each
 
+    def meta_row(s, d, r):
+        return metas[s, r // group, d, r % group : r % group + 1, :]
+
     def gather_on(s, c):
         @pl.when(s <= near)
         def _():
-            arrived(xall.at[s, c], xr.at[s - 1, c])
+            arrived(xall.at[s, c], xr.at[lax.rem(s - 1, 2), c])
 
             @pl.when(s < near)
             def _():
@@ -187,23 +214,22 @@
                     x_copy(d, s, c).start()
 
             if c == 0:
-                arrived(metas.at[s], mr.at[s - 1])
+                arrived(metas.at[s, mine], mr.at[lax.rem(s - 1, 2)])
 
                 @pl.when(s < near)
                 def _():
                     for d in (0, 1):
                         m_copy(d, s).start()
 
+                share_meta(s)
+
     def far_start(c):
         for d in (0, 1):
             far_copy(d, c).start()
-            if c == 0:
-                far_meta(d).start()
 
     def far_end():
-        arrived(metas.at[n - 1], mr.at[near])
         for c in range(cuts):
-            arrived(xall.at[n - 1, c], xr.at[near, c])
+            arrived(xall.at[n - 1, c], xr.at[2, c])
 
     def score(s, i):
         at = slice(i * wide, (i + 1) * wide)
@@ -218,7 +244,7 @@
         d, r = place(i)
         for h2 in range(ROW // LANES):
             lanes = slice(h2 * LANES, (h2 + 1) * LANES)
-            ids = metas[s, d, r : r + 1, lanes].astype(jnp.int32) - base
+            ids = meta_row(s, d, r)[:, lanes].astype(jnp.int32) - base
             ids = jnp.broadcast_to(ids, (per_half, LANES))
             owned = (ids >= 0) & (ids < experts)
             hi = jnp.where(owned, ids >> 7, -1)
@@ -237,9 +263,9 @@
         total = part[s, i : i + 1, :]
         for k in range(1, tps):
             total = total + got_ref[s, k - 1, i : i + 1, :]
-        gate = metas[s, d, lines + r : lines + r + 1, :]
+        gate = meta_row(s, d, lines + r)
         h = 0.5 * total * (1.0 + lax.erf(total * (0.5**0.5))) * gate
-        ids = metas[s, d, r : r + 1, :].astype(jnp.int32) - base
+        ids = meta_row(s, d, r).astype(jnp.int32) - base
         owned = (ids >= 0) & (ids < experts)
         code = jnp.where(owned, (ids >> 8) * per + lane_token, -1)
         lo = ids & (ROW - 1)
@@ -287,7 +313,7 @@
 
     def pass_sum(s, c):
         at = slice(c * pair, (c + 1) * pair)
-        arrived(came.at[s - 2, c], sr.at[s - 2, c])
+        arrived(came.at[s - 2, c], sr.at[lax.rem(s - 2, 2), c])
         before = came[s - 2, c].reshape(pair, width).astype(jnp.float32)
         share = mix_ref[lax.rem(s, 2), at, :]
         sent[s - 1, c] = (share + before).astype(jnp.bfloat16).reshape(2, rows, width)
@@ -295,7 +321,6 @@
             r_copy(d, s - 1, c).start()
 
     key_copy.wait()
-    far_start(0)
     for i in range(spans):
         score(0, i)
     for i in range(spans):
@@ -308,6 +333,8 @@
         for q in range(cuts):
             part_of = spans * 2 // cuts
             for i in range(q * part_of, (q + 1) * part_of):
+                if i == spans:
+                    wait_meta(t)
                 if i < spans:
                     score(t, i)
                 else:
@@ -327,30 +354,40 @@
                 score(t, i)
                 build(t - 2, i)
             gather_on(t + 1, q)
-            if q == 1:
+            reduce_on(t - 3, 1 + q)
+            if q == 0:
 
                 @pl.when(t == 3)
                 def _():
+                    for d in (0, 1):
+                        far_meta(d).start()
+
+                @pl.when(t == near - 1)
+                def _():
+                    arrived(metas.at[n - 1, mine], mr.at[2])
+                    share_meta(n - 1)
+                    far_start(2)
+
+            else:
+
+                @pl.when(t == 3)
+                def _():
+                    far_start(0)
                     far_start(1)
 
-            reduce_on(t - 3, 1 + q)
+                @pl.when(t == near - 1)
+                def _():
+                    far_start(3)
+
+        wait_meta(t)
         blend(t - 2, 0, t)
         gather_on(t + 1, 2)
-
-        @pl.when(t == near - 1)
-        def _():
-            far_start(2)
-
         reduce_on(t - 3, 3)
+
         blend(t - 2, 1, t)
         send_part(t)
         gather_on(t + 1, 3)
         reduce_on(t - 2, 0)
-
-        @pl.when(t == near - 1)
-        def _():
-            far_start(3)
-
         return carry
 
     lax.fori_loop(3, near, steady, 0)
@@ -362,6 +399,7 @@
                 score(t, i)
                 build(t - 2, i)
             pass_sum(t - 3, 1 + q)
+        wait_meta(t)
         blend(t - 2, 0, t)
         pass_sum(t - 3, 3)
         blend(t - 2, 1, t)
@@ -402,7 +440,7 @@
     places = lax.broadcasted_iota(jnp.int32, (8, LANES), 1)
     squares = jnp.zeros((8, LANES), jnp.float32)
     for c in range(cuts):
-        arrived(came.at[n - 2, c], sr.at[n - 2, c])
+        arrived(came.at[n - 2, c], sr.at[(n - 2) % 2, c])
         at = slice(c * pair, (c + 1) * pair)
         mixed = mix_ref[0, at, :] + came[n - 2, c].reshape(pair, width).astype(jnp.float32)
         mix_ref[0, at, :] = mixed
@@ -418,7 +456,8 @@
             sq_ref, sq_got.at[k - 1], ends.at[4], qr.at[0], (me, lax.rem(mine + k, tps))
         ).start()
     arrived(xall.at[pl.ds(1, n - 1)], ends.at[0])
-    arrived(metas.at[pl.ds(1, n - 1)], ends.at[1])
+    arrived(metas.at[pl.ds(1, n - 1), 0], ends.at[1])
+    arrived(metas.at[pl.ds(1, n - 1), pl.ds(0, tps - 1)], ends.at[5])
     arrived(got_ref, ends.at[2])
     arrived(sent, ends.at[3])
     arrived(sq_got, qr.at[0])
@@ -460,7 +499,7 @@
             pltpu.VMEM((experts, width), bf16),
             pltpu.VMEM((experts, width), bf16),
             pltpu.VMEM((n, cuts, 2, rows, width), bf16),
-            pltpu.VMEM((n, 2, 2 * lines, ROW), f32),
+            pltpu.VMEM((n, tps, 2, 2 * lines // tps, ROW), f32),
             pltpu.VMEM((block, experts), f32),
             pltpu.VMEM((n, 2 * lines, ROW), f32),
             pltpu.VMEM((n, tps - 1, 2 * lines, ROW), f32),
@@ -473,12 +512,13 @@
             pltpu.VMEM((picks, block), jnp.int32),
             pltpu.VMEM((picks, block), f32),
             pltpu.VMEM((1, width), f32),
-            dma((n - 1, cuts)),
+            dma((3, cuts)),
+            dma((3,)),
             dma((n - 1,)),
             dma((n,)),
-            dma((n - 1, cuts)),
+            dma((2, cuts)),
             dma((1,)),
-            dma((5,)),
+            dma((6,)),
             dma((6,)),
         ],
         compiler_params=pltpu.CompilerParams(collective_id=0, has_side_effects=True),

time: 56 us -> 55.4 us (0.989)
  no operation moved by 1% of the time
where the time goes in v4:
time: 55.4 us; the launch traced here: 55.2 us
  Pallas kernels  54.5 us (98%)
  local copies, waits for them, and re-layouts  0.71 us (1%)
    pallas_call x1, Pallas kernels, body(): pl.pallas_call(functools.partial(kernel, n, tps, picks, cycle_of(n)), out...  54.5 us

profile of v4, /device:TPU:0, one launch (start us, length us, event | category | flops | bytes accessed | tf_op | source)
XLA Modules:
  0.0 55.2 jit_solution(8436382547474583601)
XLA Ops:
  0.0 54.5 %shard_map.64 = bf16[256,512]{1,0:T(8,128)(2,1)S(1)} custom-call(bf16[256,512]{1,0:T(8,128)(2,1)} %refs_0_.1, s32[16,256]{1,0:T(8,128)} %bitcast.3, f32[16,256]{1,0:T(8,128)} %bitcast.4, bf16[4096,512]{1,0:T(8,128)(2,1)} %refs_3_.1, bf16[4096,512]{1,0:T(8,128)(2,1)} %refs_4_.1, f32[1,512]{1,0:T(1,128)} %bitcast.5), custom_call_target="tpu_custom_call" | custom-call | tf_op jit(solution)/shard_map/pallas_call | solution.py:493
  54.5 0.7 %copy.8 = bf16[256,512]{1,0:T(8,128)(2,1)} copy(bf16[256,512]{1,0:T(8,128)(2,1)S(1)} %shard_map.64) | data formatting | bytes 524288
